TPU v7x, 256 devices: a 4x2x16 block of a 4x16x16 slice. The times are simulated.
256 devices in a mesh: grp: 2 (over y), sp: 16 (over z), tp: 8 (over x, core).
Axes of the slice: x: 4, y: 2, z: 16, core: 2. Of those that a mesh axis runs over, the one named last changes fastest.
The devices are a block of a 4x16x16 slice.
Arguments:
- queries: bfloat16 [16384, 1024], P(('grp', 'sp'), 'tp'), parts along dimension 0, may hold values from -5 to 9
- keys: bfloat16 [16384, 1024], P(('grp', 'sp'), 'tp'), parts along dimension 0, may hold values from -12 to 5
- values: bfloat16 [16384, 1024], P(('grp', 'sp'), 'tp'), parts along dimension 0, may hold values from -5 to 5
- residual: bfloat16 [16384, 2048], P(('grp', 'sp')), parts along dimension 0, may hold values from -6 to 6
- out_weight: bfloat16 [1024, 2048], P('tp'), may hold values from -0.1875 to 0.1875
- post_gain: float32 [2048], replicated, may hold values from 0.1 to 1.9
- gate_weight: bfloat16 [2048, 5120], P('sp', 'tp'), may hold values from -0.125 to 0.125
- up_weight: bfloat16 [2048, 5120], P('sp', 'tp'), may hold values from -0.125 to 0.125
- down_weight: bfloat16 [5120, 2048], P('tp', 'sp'), may hold values from -0.078125 to 0.078125
- ffn_pre_gain: float32 [2048], replicated, may hold values from 0.1 to 1.9
- ffn_post_gain: float32 [2048], replicated, may hold values from 0.1 to 1.9
Outputs:
- layer_out: bfloat16 [16384, 2048], P(('grp', 'sp', 'tp')), parts along dimension 0
There are 2 independent parts, one for each index of `grp`. A program takes and returns all parts, laid end to end along the dimension named above; an argument that names none is the same for every part. Nothing has to cross between parts.
All inputs are finite; a program needn't handle non-finite values.
Results may differ from a plain program's by a relative error of at most 0.014.
Values may be sent and summed in bfloat16 or wider, within the bound.
A program may use at most 64 MiB of HBM per device.

v0:
```python
import math

import jax
import jax.numpy as jnp
from jax import lax
from jax.sharding import PartitionSpec as P

HEAD_DIM = 64


norm_eps = 1e-06


def in_one_piece(arrays, axis, dim, along):
    ends, at = ([], 0)
    for a in arrays[:-1]:
        at += a.shape[along]
        ends.append(at)
    both = jnp.concatenate(arrays, axis=along)
    return tuple(jnp.split(lax.all_gather(both, axis, axis=dim, tiled=True), ends, axis=along))


def cut_along(array, dim, devices):
    before, after = (array.shape[:dim], array.shape[dim + 1 :])
    return jnp.moveaxis(array.reshape(*before, devices, -1, *after), dim, 0)


def summed_on_arrival(array, axis, dim):
    devices = lax.axis_size(axis)
    blocks = lax.all_to_all(cut_along(array, dim, devices), axis, 0, 0, tiled=True)
    return jnp.sum(blocks.astype(jnp.float32), axis=0)


def sent_to_all(array, axis):
    devices = lax.axis_size(axis)
    return lax.all_to_all(
        jnp.broadcast_to(array[None], (devices, *array.shape)), axis, 0, 0, tiled=True
    )


def in_order(blocks, dim):
    blocks = jnp.moveaxis(blocks, 0, dim)
    dims = blocks.shape
    return blocks.reshape(*dims[:dim], dims[dim] * dims[dim + 1], *dims[dim + 2 :])


def gathered_copies(array, axis, dim):
    blocks = sent_to_all(array, axis)
    return in_order(blocks, dim)


def rms_scale(row_block, gain):
    mean_square = jnp.mean(row_block * row_block, axis=-1, keepdims=True)
    return row_block * lax.rsqrt(mean_square + norm_eps) * gain


def stick_attention(queries, keys_all, values_all, first_row, head_dim):
    tok_rows = queries.shape[0]
    head_count = queries.shape[1] // head_dim
    key_total = keys_all.shape[0]
    key_span = math.gcd(512, key_total)
    score_scale = 1.0 / math.sqrt(head_dim)
    query_heads = queries.reshape(tok_rows, head_count, head_dim)
    query_pos = first_row + lax.iota(jnp.int32, tok_rows)
    block_total = (first_row + tok_rows - 2) // key_span + 1

    def turn(turn_index, state_pair):
        output, survive = state_pair
        block_index = block_total - 1 - turn_index
        row_start = block_index * key_span
        key_block = lax.dynamic_slice_in_dim(keys_all, row_start, key_span, 0).reshape(
            key_span, head_count, head_dim
        )
        value_block = lax.dynamic_slice_in_dim(values_all, row_start, key_span, 0).reshape(
            key_span, head_count, head_dim
        )
        scores = (
            jnp.einsum("qhd,khd->hqk", query_heads, key_block, preferred_element_type=jnp.float32)
            * score_scale
        )
        key_pos = row_start + lax.iota(jnp.int32, key_span)
        strict = key_pos[None, None, :] < query_pos[None, :, None]
        fall_log = jnp.where(strict, jax.nn.log_sigmoid(-scores), 0.0)
        later_sum = lax.cumsum(fall_log, axis=2, reverse=True) - fall_log
        weights = jnp.where(
            strict, jnp.exp(jax.nn.log_sigmoid(scores) + later_sum + survive[:, :, None]), 0.0
        )
        output = output + jnp.einsum(
            "hqk,khd->hqd",
            weights.astype(jnp.bfloat16),
            value_block,
            preferred_element_type=jnp.float32,
        )
        survive = survive + jnp.sum(fall_log, axis=2)
        return (output, survive)

    initial = (
        jnp.zeros((head_count, tok_rows, head_dim), jnp.float32),
        jnp.zeros((head_count, tok_rows), jnp.float32),
    )
    output, survive = lax.fori_loop(0, block_total, turn, initial)
    return output.transpose(1, 0, 2).reshape(tok_rows, head_count * head_dim).astype(jnp.bfloat16)


def per_device(
    queries,
    keys,
    values,
    residual,
    out_weight,
    post_gain,
    gate_weight,
    up_weight,
    down_weight,
    ffn_pre_gain,
    ffn_post_gain,
):
    tok_rows = queries.shape[0]
    tp_share = lax.axis_size("tp")
    part_rows = tok_rows // tp_share
    my_rows = lax.axis_index("tp") * part_rows
    gate_full, up_full = (
        lax.all_gather(gate_weight, "sp", axis=0, tiled=True),
        lax.all_gather(up_weight, "sp", axis=0, tiled=True),
    )
    down_full = lax.all_gather(down_weight, "sp", axis=1, tiled=True)
    keys_all, values_all = in_one_piece((keys, values), "sp", 0, 1)
    attended = stick_attention(
        queries, keys_all, values_all, lax.axis_index("sp") * tok_rows, HEAD_DIM
    )
    row_block = attended
    mixed_sum = summed_on_arrival(
        jnp.dot(row_block, out_weight, preferred_element_type=jnp.float32).astype(jnp.bfloat16),
        "tp",
        0,
    )
    resid_rows = lax.dynamic_slice_in_dim(residual, my_rows, part_rows, 0).astype(jnp.float32)
    first_mine = resid_rows + rms_scale(mixed_sum, post_gain)
    mine_in = rms_scale(first_mine, ffn_pre_gain).astype(jnp.bfloat16)
    ffn_in = gathered_copies(mine_in, "tp", 0)
    gate_sum = jnp.dot(ffn_in, gate_full, preferred_element_type=jnp.float32)
    up_sum = jnp.dot(ffn_in, up_full, preferred_element_type=jnp.float32)
    hidden = (jax.nn.silu(gate_sum) * up_sum).astype(jnp.bfloat16)
    row_block = hidden
    ffn_out = summed_on_arrival(
        jnp.dot(row_block, down_full, preferred_element_type=jnp.float32).astype(jnp.bfloat16),
        "tp",
        0,
    )
    result = first_mine + 0.5 * rms_scale(ffn_out, ffn_post_gain)
    return result.astype(jnp.bfloat16)


def solution(mesh):
    in_specs = (
        P(("grp", "sp"), "tp"),
        P(("grp", "sp"), "tp"),
        P(("grp", "sp"), "tp"),
        P(("grp", "sp"), None),
        P("tp", None),
        P(),
        P("sp", "tp"),
        P("sp", "tp"),
        P("tp", "sp"),
        P(),
        P(),
    )
    out_specs = P(("grp", "sp", "tp"), None)
    return jax.shard_map(
        per_device, mesh=mesh, in_specs=in_specs, out_specs=out_specs, check_vma=False
    )
```

profile of v0, /device:TPU:33, one launch (start us, length us, event | category | flops | bytes accessed | tf_op | source)
XLA Modules:
  0.0 542.8 jit_solution(2546121438014420880)
XLA Ops:
  6.5 0.0 copy-start
  6.6 0.0 all-gather.5.cloned.1.call-start
  6.6 1.1 copy.15
  7.6 1.0 copy.16
  8.6 0.7 pad_maximum_fusion
  9.4 0.1 all-gather.5.cloned.1.call-update
  9.4 0.1 all-gather.7.cloned.1.call-start
  9.5 0.7 all-gather.7.cloned.1.call-update
  10.2 0.1 all-gather.11.cloned.1.call-start
  10.3 0.7 all-gather.11.cloned.1.call-update
  11.0 1.0 copy.17
  12.1 79.2 %all-gather.5.cloned.1.call-done = bf16[8192,256]{0,1:T(8,128)(2,1)} async-done(((bf16[512,256]{0,1:T(8,128)(2,1)}), bf16[8192,256]{0,1:T(8,128)(2,1)}) %all-gather.5.cloned.1.call-update) | async-done | bytes 4194320 | tf_op jit(solution)/shard_map/all_gather | solution.py:20
  91.2 4.7 fusion.19
  96.0 19.8 %while.15 = (s32[]{:T(128)}, f32[2,512,64]{1,2,0:T(8,128)S(1)}, f32[2,512]{1,0:T(2,128)S(1)}, s32[]{:T(128)}, s32[]{:T(128)}, /*index=5*/bf16[8192,128]{0,1:T(8,...) while((s32[]{:T(128)}, f32[2,512,64]{1,2,0:T(8,128)S(1)}, ...), condition=%wide.region_4.5_spmd.clone, body=%wide.region_0.4_spmd.clone.sunk | while | flops 218447872 | bytes 33833192 | solution.py:101
  96.0 1.0 constant_dynamic-slice_fusion.3
  97.0 0.2 broadcast_compare_fusion.2
  97.2 3.1 fusion.45
  100.4 9.6 %fusion.46 = f32[2,512,4,128]{1,2,3,0:T(4,128)S(1)} fusion(f32[2,512,4,128]{1,3,2,0:T(8,128)S(1)} %bitcast.72), kind=kOutput, calls=%fused_computation.19.clone.1 | output fusion | flops 66584576 | bytes 4194304 | tf_op jit(solution)/shard_map/reduce-window.4
  110.1 0.4 broadcast_add_fusion.2
  110.4 0.0 copy-start.1
  110.4 0.6 copy.24
  111.1 1.0 copy-done.1
  112.0 3.3 fusion.47
  115.3 0.3 convolution_add_fusion.2
  115.8 0.0 copy-done
  115.8 2.1 convolution_convert_fusion
  117.9 14.3 %all-to-all-start = ((bf16[8,64,2048]{2,1,0:T(8,128)(2,1)}), bf16[8,64,2048]{2,1,0:T(8,128)(2,1)S(1)}, u32[]{:S(2)}, u32[]{:S(2)}) async-start(bf16[8,64,2048]{2,1,0:T(8,128)(2,1)} %bitcast.74), calls=%async_computation | async-start | bytes 4194304 | tf_op jit(solution)/shard_map/all_to_all | solution.py:30
  132.2 0.1 all-gather.9.cloned.1.call-start
  132.2 0.6 all-gather.9.cloned.1.call-update
  132.8 25.6 %all-to-all-done = bf16[8,64,2048]{2,1,0:T(8,128)(2,1)S(1)} async-done(((bf16[8,64,2048]{2,1,0:T(8,128)(2,1)}), bf16[8,64,2048]{2,1,0:T(8,128)(2,1)S(1)}, u32[]{:S(2)}, u32[]{:S(2)}) %all-to-all-start) | async-done | bytes 2097184 | tf_op jit(solution)/shard_map/all_to_all | solution.py:30
  158.4 0.3 convert_reduce_fusion.1
  158.7 0.1 multiply_reduce_fusion.2
  158.9 0.0 copy-done.2
  158.9 1.2 multiply_reduce_fusion.1
  160.1 0.0 copy-done.3
  160.1 1.1 multiply_convert_fusion
  161.3 1.6 broadcast_in_dim.40
  162.9 4.5 all-to-all-start.1
  167.4 26.3 %all-to-all-done.1 = bf16[8,64,2048]{2,1,0:T(8,128)(2,1)S(1)} async-done(((bf16[8,64,2048]{2,1,0:T(8,128)(2,1)}), bf16[8,64,2048]{2,1,0:T(8,128)(2,1)S(1)}, u32[]{:S(2)}, u32[]{:S(2)}) %all-to-all-start.1) | async-done | bytes 2097184 | tf_op jit(solution)/shard_map/all_to_all | solution.py:36
  193.7 4.6 fusion.20
  198.3 41.7 %all-gather.11.cloned.1.call-done = bf16[640,2048]{1,0:T(8,128)(2,1)} async-done(((bf16[640,128]{1,0:T(8,128)(2,1)}), bf16[640,2048]{1,0:T(8,128)(2,1)}) %all-gather.11.cloned.1.call-update) | async-done | bytes 2621456 | tf_op jit(solution)/shard_map/all_gather | solution.py:126
  240.0 244.5 %all-gather.9.cloned.1.call-done = bf16[2048,640]{1,0:T(8,128)(2,1)} async-done(((bf16[128,640]{1,0:T(8,128)(2,1)}), bf16[2048,640]{1,0:T(8,128)(2,1)}) %all-gather.9.cloned.1.call-update) | async-done | bytes 2621456 | tf_op jit(solution)/shard_map/all_gather | solution.py:124
  484.5 8.3 %convolution_convert_fusion.1 = bf16[512,2048]{1,0:T(8,128)(2,1)} fusion(bf16[640,2048]{1,0:T(8,128)(2,1)} %all-gather.11.cloned.1.call-done, bf16[512,2048]{1,0:T(8,128)(2,1)S(1)} %bitcast.77, bf16[2048,640]{1,0:T(8,128)(2,1)} %all-gather.9.cloned.1.call-done, f32[512,640]{1,0:T(8,128)} %fusion.20), kind=kOutput, calls=%fused_computation.33 | convolution fusion | flops 2687369216 | bytes 10747904 | tf_op jit(solution)/shard_map/dot_general | solution.py:146
  492.8 40.9 %all_to_all.15 = bf16[8,64,2048]{2,1,0:T(8,128)(2,1)S(1)} all-to-all(bf16[8,64,2048]{2,1,0:T(8,128)(2,1)} %bitcast.78), channel_id=1, replica_groups=mesh['grp'=2,'sp'=16,'tp'=8] {'tp'}, dimensions={0} | all-to-all | bytes 4194304 | tf_op jit(solution)/shard_map/all_to_all | solution.py:30
  533.7 0.4 convert_reduce_fusion
  534.1 0.1 multiply_reduce_fusion
  534.2 0.2 copy-done.4
  534.4 1.9 add_convert_fusion
  (15 shorter events, 0.1 us)
Async XLA Ops:
  6.5 109.3 %copy-start = (bf16[128,2048]{1,0:T(8,128)(2,1)S(1)}, bf16[128,2048]{1,0:T(8,128)(2,1)}, u32[]{:S(2)}) copy-start(bf16[128,2048]{1,0:T(8,128)(2,1)} %param.17) | copy-start | bytes 1572868
  6.6 84.7 %all-gather.5.cloned.1.call-start = ((), (), s32[]{:S(2)}) async-start(), calls=%async_computation.3 | async-start | bytes 4456448 | tf_op jit(solution)/shard_map/all_gather | solution.py:20
  9.4 157.9 %all-gather.7.cloned.1.call-start = ((), (), s32[]{:S(2)}) async-start(), calls=%async_computation.4 | async-start | bytes 2785280 | tf_op jit(solution)/shard_map/all_gather | solution.py:123
  10.2 229.8 %all-gather.11.cloned.1.call-start = ((), (), s32[]{:S(2)}) async-start(), calls=%async_computation.6 | async-start | bytes 2785280 | tf_op jit(solution)/shard_map/all_gather | solution.py:126
  110.4 1.6 copy-start.1
  117.9 40.5 %all-to-all-start = ((bf16[8,64,2048]{2,1,0:T(8,128)(2,1)}), bf16[8,64,2048]{2,1,0:T(8,128)(2,1)S(1)}, u32[]{:S(2)}, u32[]{:S(2)}) async-start(bf16[8,64,2048]{2,1,0:T(8,128)(2,1)} %bitcast.74), calls=%async_computation | async-start | bytes 4194304 | tf_op jit(solution)/shard_map/all_to_all | solution.py:30
  132.2 26.7 %copy-start.2 = (f32[2048]{0:T(1024)S(1)}, f32[2048]{0:T(1024)}, u32[]{:S(2)}) copy-start(f32[2048]{0:T(1024)} %param.18) | copy-start | bytes 24580
  132.2 28.0 %copy-start.3 = (f32[2048]{0:T(1024)S(1)}, f32[2048]{0:T(1024)}, u32[]{:S(2)}) copy-start(f32[2048]{0:T(1024)} %param.22) | copy-start | bytes 24580
  132.2 352.4 %all-gather.9.cloned.1.call-start = ((), (), s32[]{:S(2)}) async-start(), calls=%async_computation.5 | async-start | bytes 2785280 | tf_op jit(solution)/shard_map/all_gather | solution.py:124
  162.9 30.8 %all-to-all-start.1 = ((bf16[8,64,2048]{2,1,0:T(8,128)(2,1)}), bf16[8,64,2048]{2,1,0:T(8,128)(2,1)S(1)}, u32[]{:S(2)}, u32[]{:S(2)}) async-start(bf16[8,64,2048]{2,1,0:T(8,128)(2,1)} %broadcast_in_dim.40), calls=%async_computation.1 | async-start | bytes 4194304 | tf_op jit(solution)/shard_map/all_to_all | solution.py:36
  533.7 0.7 copy-start.4
Sparse Core Ops, SparseCore 0:
  9.5 81.6 all-gather.4
  93.0 69.1 all-gather.6
  164.0 75.9 all-gather.10
  241.7 242.8 all-gather.8
where the time goes:
time: 544 us; the launch traced here: 543 us
  waiting for transfers between devices  419 us (77%)
  blocking collectives  40.9 us (8%)
  other arithmetic  19.6 us (4%)
  starting transfers between devices  18.9 us (3%)
  matrix products  18.4 us (3%)
  between operations  13.3 us (2%)
  local copies, waits for them, and re-layouts  12.2 us (2%)
    all_gather x1, waiting for transfers between devices, per_device(): lax.all_gather(up_weight, 'sp', axis=0, tiled=True)  245 us
    all_gather x1, waiting for transfers between devices, in_one_piece(): lax.all_gather(both, axis, axis=dim, tiled=True)  79.2 us
    all_gather x1, waiting for transfers between devices, per_device(): down_full = lax.all_gather(down_weight, 'sp', axis=1, tiled=True)  41.7 us
    all_to_all x1, blocking collectives, summed_on_arrival(): lax.all_to_all(cut_along(array, dim, devices), axis, 0, 0, tiled=True)  40.9 us
    all_to_all x1, waiting for transfers between devices, sent_to_all(): lax.all_to_all(jnp.broadcast_to(array[None], (devices, *array.shape)), ax...  26.3 us
    all_to_all x1, waiting for transfers between devices, summed_on_arrival(): lax.all_to_all(cut_along(array, dim, devices), axis, 0, 0, tiled=True)  25.6 us
    all_to_all x1, starting transfers between devices, summed_on_arrival(): lax.all_to_all(cut_along(array, dim, devices), axis, 0, 0, tiled=True)  14.3 us
  transfers between devices with their start and end apart: 6, of which 5 were waited for; matrix products, arithmetic and copies ran while one was open for 7% of the time, Pallas kernels for 0%

commit v1 on v0

v1 whole, which is shorter than its diff:
```python
import functools

import jax
import jax.numpy as jnp
from jax import lax
from jax.experimental import pallas as pl
from jax.experimental.pallas import tpu as pltpu
from jax.sharding import PartitionSpec as P

HEAD_DIM = 64
norm_eps = 1e-06
MESH = pl.DeviceIdType.MESH
F32 = jnp.float32
BF16 = jnp.bfloat16


def rcopy(src, dst, send_sem, recv_sem, device):
    return pltpu.make_async_remote_copy(
        src_ref=src, dst_ref=dst, send_sem=send_sem, recv_sem=recv_sem,
        device_id=device, device_id_type=MESH,
    )


def layer_kernel(
    n, m,
    q_ref, k_ref, v_ref, res_ref, wo_ref, pg_ref, gate_ref, up_ref, down_ref, prg_ref, fg_ref,
    out_ref,
    kall, vall, gall, uall, dall, qm, tri, acc, acc_low, lost, att, sbuf, rbuf, res_v, first, x_all, hidden,
    fbuf, rb, ff,
    ring_send, ring_recv, rs_send, rs_recv, ag_send, ag_recv, fs_send, fs_recv, res_sem,
):
    s = lax.axis_index("sp")
    me = lax.axis_index("tp")
    nxt, prv = lax.rem(s + 1, n), lax.rem(s + n - 1, n)
    toks, width = q_ref.shape
    heads = width // HEAD_DIM
    d_rows = gate_ref.shape[0]
    f_half = down_ref.shape[0] // 2
    cols = down_ref.shape[1]
    d_model = wo_ref.shape[1]
    part = toks // m
    kc = min(256, toks)
    qt = min(128, toks)
    near, far = n // 2 - 1, n // 2

    barrier = pltpu.get_barrier_semaphore()
    for z in (nxt, prv):
        pl.semaphore_signal(barrier, inc=1, device_id={"sp": z}, device_id_type=MESH)
    for d in range(1, m):
        pl.semaphore_signal(barrier, inc=1, device_id={"tp": lax.rem(me + d, m)}, device_id_type=MESH)
    pl.semaphore_wait(barrier, m + 1)

    streams = [
        (k_ref, lambda o: kall.at[o], (far, near)),
        (v_ref, lambda o: vall.at[o], (far, near)),
        (gate_ref, lambda o: gall.at[pl.ds(pl.multiple_of(o * d_rows, d_rows), d_rows), :], (near, far)),
        (up_ref, lambda o: uall.at[pl.ds(pl.multiple_of(o * d_rows, d_rows), d_rows), :], (near, far)),
        (down_ref.at[pl.ds(0, f_half), :], lambda o: dall.at[o, pl.ds(0, f_half), :], (far, near)),
        (down_ref.at[pl.ds(f_half, f_half), :], lambda o: dall.at[o, pl.ds(f_half, f_half), :], (far, near)),
    ]

    def origin_out(way, k):
        return lax.rem(s + n - k, n) if way == 0 else lax.rem(s + k, n)

    def origin_in(way, k):
        return lax.rem(s + n - 1 - k, n) if way == 0 else lax.rem(s + 1 + k, n)

    def out_copy(i, way, k):
        own, place, _ = streams[i]
        at = place(origin_out(way, k))
        src = own if isinstance(k, int) and k == 0 else at
        return rcopy(src, at, ring_send.at[i, way, k], ring_recv.at[i, way, k], {"sp": nxt if way == 0 else prv})

    def in_copy(i, way, k):
        at = streams[i][1](origin_in(way, k))
        return rcopy(at, at, ring_send.at[i, way, k], ring_recv.at[i, way, k], {"sp": prv if way == 0 else nxt})

    def start_group(group):
        for i in group:
            for way in (0, 1):
                if streams[i][2][way]:
                    out_copy(i, way, 0).start()

    def service(group, k):
        for i in group:
            for way in (0, 1):
                hops = streams[i][2][way]
                if k < hops:
                    in_copy(i, way, k).wait_recv()
                    if k + 1 < hops:
                        out_copy(i, way, k + 1).start()

    def drain(group):
        for i in group:
            for way in (0, 1):
                for k in range(streams[i][2][way]):
                    out_copy(i, way, k).wait_send()

    KV, GU, DN = (0, 1), (2, 3), (4, 5)

    @pl.when(s < n - 1)
    def _():
        for i in KV:
            out_copy(i, 0, 0).start()

    @pl.when(s < near)
    def _():
        for i in KV:
            out_copy(i, 1, 0).start()

    res_copy = pltpu.make_async_copy(res_ref.at[pl.ds(pl.multiple_of(me * part, part), part), :], res_v, res_sem)
    res_copy.start()

    lane_head = lax.broadcasted_iota(jnp.int32, (toks, width), 1) // HEAD_DIM
    scaled = q_ref[...].astype(F32) * (1.0 / HEAD_DIM**0.5)
    for h in range(heads):
        qm[h] = jnp.where(lane_head == h, scaled, 0.0).astype(BF16)
    tri[...] = jnp.where(
        lax.broadcasted_iota(jnp.int32, (kc, kc), 0) > lax.broadcasted_iota(jnp.int32, (kc, kc), 1), 1.0, 0.0
    ).astype(BF16)
    acc_low[...] = jnp.zeros_like(acc_low)
    gall[pl.ds(pl.multiple_of(s * d_rows, d_rows), d_rows), :] = gate_ref[...]
    uall[pl.ds(pl.multiple_of(s * d_rows, d_rows), d_rows), :] = up_ref[...]

    def attend(keys, vals, mode):
        def tile(i, carry_in):
            rows = pl.ds(pl.multiple_of(i * qt, qt), qt)
            for h in range(heads):
                qtile = qm[h, rows, :]
                gone = lost[h, rows, :] if mode == "high" else jnp.zeros((qt, 1), F32)
                out = jnp.zeros((qt, width), F32)
                for c in reversed(range(toks // kc)):
                    z = lax.dot_general(
                        qtile, keys[pl.ds(c * kc, kc), :], (((1,), (1,)), ((), ())), preferred_element_type=F32
                    )
                    soft = jnp.maximum(z, 0.0) + jnp.log(1.0 + jnp.exp(-jnp.abs(z)))
                    take = z - soft
                    if mode == "own":
                        key_pos = c * kc + lax.broadcasted_iota(jnp.int32, (qt, kc), 1)
                        strict = key_pos < i * qt + lax.broadcasted_iota(jnp.int32, (qt, kc), 0)
                        soft = jnp.where(strict, soft, 0.0)
                    head = soft.astype(BF16)
                    rest = (soft - head.astype(F32)).astype(BF16)
                    later = jnp.dot(head, tri[...], preferred_element_type=F32) + jnp.dot(
                        rest, tri[...], preferred_element_type=F32
                    )
                    weight = jnp.exp(take - later - gone)
                    if mode == "own":
                        weight = jnp.where(strict, weight, 0.0)
                    out = out + jnp.dot(
                        weight.astype(BF16), vals[pl.ds(c * kc, kc), :], preferred_element_type=F32
                    )
                    gone = gone + later[:, 0:1] + soft[:, 0:1]
                if mode == "own":
                    acc[h, rows, :] = out
                    lost[h, rows, :] = gone
                elif mode == "high":
                    acc[h, rows, :] = acc[h, rows, :] + out
                    lost[h, rows, :] = gone
                else:
                    acc_low[h, rows, :] = acc_low[h, rows, :] * jnp.exp(-gone) + out
            return carry_in

        lax.fori_loop(0, toks // qt, tile, 0)

    attend(k_ref, v_ref, "own")

    def kv_step(k, carry_in):
        up_need = s - 1 - k >= 0
        wrap = lax.rem(s + 1 + k, n)
        down_need = jnp.logical_and(k < near, wrap < near)
        for i in KV:
            @pl.when(up_need)
            def _():
                in_copy(i, 0, k).wait_recv()

                @pl.when(jnp.logical_and(k + 1 < far, s < n - 1))
                def _():
                    out_copy(i, 0, k + 1).start()

            @pl.when(down_need)
            def _():
                in_copy(i, 1, k).wait_recv()

                @pl.when(k + 1 < near)
                def _():
                    out_copy(i, 1, k + 1).start()

        @pl.when(k == far - 2)
        def _():
            start_group(GU)

        @pl.when(up_need)
        def _():
            o = origin_in(0, k)
            attend(kall.at[o], vall.at[o], "high")

        @pl.when(jnp.logical_and(down_need, wrap < s))
        def _():
            attend(kall.at[wrap], vall.at[wrap], "low")

        return carry_in

    lax.fori_loop(0, far, kv_step, 0)

    whole = [acc[h] + acc_low[h] * jnp.exp(-lost[h]) for h in range(heads)]
    joined = whole[0]
    for h in range(1, heads):
        joined = jnp.where(lane_head == h, whole[h], joined)
    att[...] = joined.astype(BF16)
    nc = min(512, d_model)
    for c in range(d_model // nc):
        sbuf[:, pl.ds(c * nc, nc)] = jnp.dot(
            att[...], wo_ref[:, pl.ds(c * nc, nc)], preferred_element_type=F32
        ).astype(BF16)

    def rs_copy(d):
        p = lax.rem(me + d, m)
        return rcopy(
            sbuf.at[pl.ds(pl.multiple_of(p * part, part), part), :], rbuf.at[d - 1],
            rs_send.at[d - 1], rs_recv.at[d - 1], {"tp": p},
        )

    def ag_copy(d):
        mine = x_all.at[pl.ds(pl.multiple_of(me * part, part), part), :]
        return rcopy(mine, mine, ag_send.at[d - 1], ag_recv.at[d - 1], {"tp": lax.rem(me + d, m)})

    def ag_in(d):
        p = lax.rem(me + m - d, m)
        at = x_all.at[pl.ds(pl.multiple_of(p * part, part), part), :]
        return rcopy(at, at, ag_send.at[d - 1], ag_recv.at[d - 1], {"tp": p})

    for d in range(1, m):
        rs_copy(d).start()

    def norm(v, gain):
        mean_square = jnp.mean(v * v, axis=-1, keepdims=True)
        return v * lax.rsqrt(mean_square + norm_eps) * gain

    third = (far + 1) // 3
    for k in range(third):
        service(GU, k)
    for d in range(1, m):
        rs_copy(d).wait()
    mixed = sbuf[pl.ds(pl.multiple_of(me * part, part), part), :].astype(F32)
    for d in range(1, m):
        mixed = mixed + rbuf[d - 1].astype(F32)
    res_copy.wait()
    first[...] = res_v[...].astype(F32) + norm(mixed, pg_ref[...])
    x_all[pl.ds(pl.multiple_of(me * part, part), part), :] = norm(first[...], prg_ref[...]).astype(BF16)
    for d in range(1, m):
        ag_copy(d).start()
    for k in range(third, far):
        if k == far - 1:
            start_group(DN)
        service(GU, k)
    for d in range(1, m):
        ag_in(d).wait_recv()

    mt = min(256, toks)

    def ffn_tile(i, carry_in):
        rows = pl.ds(pl.multiple_of(i * mt, mt), mt)
        g = jnp.dot(x_all[rows, :], gall[...], preferred_element_type=F32)
        u = jnp.dot(x_all[rows, :], uall[...], preferred_element_type=F32)
        hidden[rows, :] = (g / (1.0 + jnp.exp(-g)) * u).astype(BF16)
        return carry_in

    lax.fori_loop(0, toks // mt, ffn_tile, 0)

    def fs_copy(c, wide, d):
        p = lax.rem(me + d, m)
        return rcopy(
            fbuf.at[c, pl.ds(pl.multiple_of(p * part, part), part), pl.ds(0, wide)], rb.at[c, d - 1, :, pl.ds(0, wide)],
            fs_send.at[c, d - 1], fs_recv.at[c, d - 1], {"tp": p},
        )

    def chunk_origins(c):
        if c == 0:
            return [s]
        return [origin_in(way, c - 1) for way in (0, 1) if c - 1 < streams[DN[0]][2][way]]

    for c in range(far + 1):
        if c:
            service(DN, c - 1)
        origins = chunk_origins(c)
        tiles = [down_ref[...] if c == 0 else dall[o] for o in origins]
        wide = cols * len(tiles)
        both = tiles[0] if len(tiles) == 1 else jnp.concatenate(tiles, axis=1)
        fbuf[c, :, pl.ds(0, wide)] = jnp.dot(hidden[...], both, preferred_element_type=F32).astype(BF16)
        for d in range(1, m):
            fs_copy(c, wide, d).start()

    square = jnp.zeros((part, 1), F32)
    for c in range(far + 1):
        origins = chunk_origins(c)
        wide = cols * len(origins)
        for d in range(1, m):
            fs_copy(c, wide, d).wait()
        total = fbuf[c, pl.ds(pl.multiple_of(me * part, part), part), pl.ds(0, wide)].astype(F32)
        for d in range(1, m):
            total = total + rb[c, d - 1, :, pl.ds(0, wide)].astype(F32)
        square = square + jnp.sum(total * total, axis=-1, keepdims=True)
        for j, o in enumerate(origins):
            ff[o] = total[:, j * cols : (j + 1) * cols]
    scale = lax.rsqrt(square / d_model + norm_eps)
    for o in range(n):
        at = pl.ds(o * cols, cols)
        out_ref[:, at] = (first[:, at] + 0.5 * (ff[o] * scale * fg_ref[:, at])).astype(out_ref.dtype)

    for d in range(1, m):
        ag_copy(d).wait_send()

    def kv_drain(k, carry_in):
        for i in KV:
            @pl.when(jnp.logical_and(s < n - 1, s - k >= 0))
            def _():
                out_copy(i, 0, k).wait_send()

            @pl.when(jnp.logical_and(k < near, lax.rem(s + k, n) < near))
            def _():
                out_copy(i, 1, k).wait_send()

        return carry_in

    lax.fori_loop(0, far, kv_drain, 0)
    drain(GU)
    drain(DN)


def solution(mesh):
    n, m = mesh.shape["sp"], mesh.shape["tp"]

    def per_device(q, k, v, residual, wo, pg, gate, up, down, prg, fg):
        toks, width = q.shape
        d_model = wo.shape[1]
        f_loc = gate.shape[1]
        heads = width // HEAD_DIM
        part = toks // m
        cols = down.shape[1]
        far = n // 2
        chunks = far + 1
        kc = min(256, toks)
        vm, dma = pltpu.VMEM, pltpu.SemaphoreType.DMA
        in_vmem = pl.BlockSpec(memory_space=vm)
        specs = [in_vmem] * 11
        specs[3] = pl.BlockSpec(memory_space=pl.ANY)
        flops = 2 * toks * (n * toks * width * 4 + width * d_model + 3 * d_model * f_loc)
        return pl.pallas_call(
            functools.partial(layer_kernel, n, m),
            out_shape=jax.ShapeDtypeStruct((part, d_model), BF16),
            in_specs=specs,
            out_specs=in_vmem,
            scratch_shapes=[
                vm((n, toks, width), BF16),
                vm((n, toks, width), BF16),
                vm((d_model, f_loc), BF16),
                vm((d_model, f_loc), BF16),
                vm((n, f_loc, cols), BF16),
                vm((heads, toks, width), BF16),
                vm((kc, kc), BF16),
                vm((heads, toks, width), F32),
                vm((heads, toks, width), F32),
                vm((heads, toks, 1), F32),
                vm((toks, width), BF16),
                vm((toks, d_model), BF16),
                vm((m - 1, part, d_model), BF16),
                vm((part, d_model), BF16),
                vm((part, d_model), F32),
                vm((toks, d_model), BF16),
                vm((toks, f_loc), BF16),
                vm((chunks, toks, 2 * cols), BF16),
                vm((chunks, m - 1, part, 2 * cols), BF16),
                vm((n, part, cols), F32),
                dma((6, 2, far)),
                dma((6, 2, far)),
                dma((m - 1,)),
                dma((m - 1,)),
                dma((m - 1,)),
                dma((m - 1,)),
                dma((chunks, m - 1)),
                dma((chunks, m - 1)),
                dma,
            ],
            compiler_params=pltpu.CompilerParams(
                collective_id=0, has_side_effects=True, vmem_limit_bytes=60 * 1024 * 1024
            ),
            cost_estimate=pl.CostEstimate(flops=flops, bytes_accessed=4 * toks * d_model, transcendentals=0),
        )(q, k, v, residual, wo, pg.reshape(1, -1), gate, up, down, prg.reshape(1, -1), fg.reshape(1, -1))

    in_specs = (
        P(("grp", "sp"), "tp"),
        P(("grp", "sp"), "tp"),
        P(("grp", "sp"), "tp"),
        P(("grp", "sp"), None),
        P("tp", None),
        P(),
        P("sp", "tp"),
        P("sp", "tp"),
        P("tp", "sp"),
        P(),
        P(),
    )
    out_specs = P(("grp", "sp", "tp"), None)
    return jax.shard_map(per_device, mesh=mesh, in_specs=in_specs, out_specs=out_specs, check_vma=False)
```

time: 544 us -> 190 us (0.35)
  waiting for transfers between devices: 419 us -> 0 us
  Pallas kernels: 0 us -> 188 us
  blocking collectives: 40.9 us -> 0 us
  other arithmetic: 19.6 us -> 0 us
  starting transfers between devices: 18.9 us -> 0 us
  matrix products: 18.4 us -> 0 us
  between operations: 13.3 us -> 0.01 us
  local copies, waits for them, and re-layouts: 12.2 us -> 1.67 us
    all_gather x4 -> x0, waiting for transfers between devices: 365 us -> none  [the longest x1 245 us: per_device(): lax.all_gather(up_weight, 'sp', axis=0, tiled=True)]
    pallas_call x0 -> x1, Pallas kernels: none -> 188 us  [per_device(): pl.pallas_call(functools.partial(layer_kernel, n, m), out_shape=jax.Shape...]
    all_to_all x2 -> x0, waiting for transfers between devices: 51.9 us -> none  [the longest x1 26.3 us: sent_to_all(): lax.all_to_all(jnp.broadcast_to(array[None], (devices, *array.shape)), ax...]
    all_to_all x1 -> x0, blocking collectives: 40.9 us -> none  [summed_on_arrival(): lax.all_to_all(cut_along(array, dim, devices), axis, 0, 0, tiled=True)]
    all_to_all x2 -> x0, starting transfers between devices: 18.7 us -> none  [the longest x1 14.3 us: summed_on_arrival(): lax.all_to_all(cut_along(array, dim, devices), axis, 0, 0, tiled=True)]
    dot_general x5 -> x0, matrix products: 18.4 us -> none  [the longest x1 8.31 us: per_device(): jnp.dot(row_block, down_full, preferred_element_type=jnp.float32)]
    another operation x3 -> x0, other arithmetic: 10 us -> none
    convert_element_type x4 -> x0, other arithmetic: 6.31 us -> none  [the longest x1 3.27 us: turn(): weights.astype(jnp.bfloat16)]
  transfers between devices with their start and end apart: 6 -> 0, of which waited for: 5 -> 0; matrix products, arithmetic and copies ran while one was open for 7% -> 0% of each run, Pallas kernels for 0% -> 0%
where the time goes in v1:
time: 190 us
  Pallas kernels  188 us (99%)
    pallas_call x1, Pallas kernels, per_device(): pl.pallas_call(functools.partial(layer_kernel, n, m), out_shape=jax.Shape...  188 us

profile of v1, /device:TPU:33, one launch (start us, length us, event | category | flops | bytes accessed | tf_op | source)
XLA Modules:
  0.0 189.6 jit_solution(14392743292067863713)
XLA Ops:
  0.0 187.9 %shard_map.109 = bf16[64,2048]{1,0:T(8,128)(2,1)} custom-call(bf16[512,128]{1,0:T(8,128)(2,1)} %q_ref.1, bf16[512,128]{1,0:T(8,128)(2,1)} %k_ref.1, bf16[512,128]{1,0:T(8,128)(2,1)} %v_ref.1, bf16[512,2048]{1,0:T(8,128)(2,1)} %res_ref.1, bf16[128,2048]{1,0:T(8,128)(2,1)} %wo_ref.1, f32[1,2048]{1,0:T(1,128)} %bitcast.3, bf16[128,640]{1,0:T(8,128)(2,1)} %gate_ref.1, ...), custom_call_target="tpu_custom_call" | custom-call | flops 8589934592 | bytes 4194304 | tf_op jit(solution)/shard_map/pallas_call | solution.py:349
  187.9 1.7 copy.13

commit v2 on v1

--- a/solution.py
+++ b/solution.py
@@ -9,6 +9,7 @@
 
 HEAD_DIM = 64
 norm_eps = 1e-06
+LOG2_E = 1.4426950408889634
 MESH = pl.DeviceIdType.MESH
 F32 = jnp.float32
 BF16 = jnp.bfloat16
@@ -22,13 +23,14 @@
 
 
 def layer_kernel(
-    n, m,
+    groups, n, m,
     q_ref, k_ref, v_ref, res_ref, wo_ref, pg_ref, gate_ref, up_ref, down_ref, prg_ref, fg_ref,
     out_ref,
-    kall, vall, gall, uall, dall, qm, tri, acc, acc_low, lost, att, sbuf, rbuf, res_v, first, x_all, hidden,
+    kall, vall, gall, uall, dall, qm, tri, acc, acc_low, lost, att, sbuf, pbuf, tbuf, hbuf, cbuf, res_v, first, x_all, hidden,
     fbuf, rb, ff,
-    ring_send, ring_recv, rs_send, rs_recv, ag_send, ag_recv, fs_send, fs_recv, res_sem,
+    ring_send, ring_recv, cross_send, cross_recv, rs_send, rs_recv, ag_send, ag_recv, fs_send, fs_recv, res_sem,
 ):
+    g = lax.axis_index("grp")
     s = lax.axis_index("sp")
     me = lax.axis_index("tp")
     nxt, prv = lax.rem(s + 1, n), lax.rem(s + n - 1, n)
@@ -40,7 +42,7 @@
     d_model = wo_ref.shape[1]
     part = toks // m
     kc = min(256, toks)
-    qt = min(128, toks)
+    qt = min(256, toks)
     near, far = n // 2 - 1, n // 2
 
     barrier = pltpu.get_barrier_semaphore()
@@ -48,16 +50,65 @@
         pl.semaphore_signal(barrier, inc=1, device_id={"sp": z}, device_id_type=MESH)
     for d in range(1, m):
         pl.semaphore_signal(barrier, inc=1, device_id={"tp": lax.rem(me + d, m)}, device_id_type=MESH)
-    pl.semaphore_wait(barrier, m + 1)
+    sides = sorted({1 % groups, groups - 1} - {0})
+    for d in sides:
+        pl.semaphore_signal(barrier, inc=1, device_id={"grp": lax.rem(g + d, groups)}, device_id_type=MESH)
+    pl.semaphore_wait(barrier, m + 1 + len(sides))
+
+    d_half = d_rows // 2
+
+    def w_rows(ref, begin, size):
+        return lambda o: ref.at[pl.ds(pl.multiple_of(o * d_rows + begin, size), size), :]
 
     streams = [
-        (k_ref, lambda o: kall.at[o], (far, near)),
-        (v_ref, lambda o: vall.at[o], (far, near)),
-        (gate_ref, lambda o: gall.at[pl.ds(pl.multiple_of(o * d_rows, d_rows), d_rows), :], (near, far)),
-        (up_ref, lambda o: uall.at[pl.ds(pl.multiple_of(o * d_rows, d_rows), d_rows), :], (near, far)),
-        (down_ref.at[pl.ds(0, f_half), :], lambda o: dall.at[o, pl.ds(0, f_half), :], (far, near)),
-        (down_ref.at[pl.ds(f_half, f_half), :], lambda o: dall.at[o, pl.ds(f_half, f_half), :], (far, near)),
+        (k_ref, lambda o: kall.at[o], (far, near), False),
+        (v_ref, lambda o: vall.at[o], (far, near), False),
+        (gate_ref, w_rows(gall, 0, d_rows), (near, far), True),
+        (up_ref.at[pl.ds(0, d_half), :], w_rows(uall, 0, d_half), (near, far), False),
+        (up_ref.at[pl.ds(d_half, d_half), :], w_rows(uall, d_half, d_half), (near, far), True),
+        (down_ref.at[pl.ds(0, f_half), :], lambda o: dall.at[o, pl.ds(0, f_half), :], (far, near), False),
+        (down_ref.at[pl.ds(f_half, f_half), :], lambda o: dall.at[o, pl.ds(f_half, f_half), :], (far, near), False),
     ]
+    split = [i for i, stream in enumerate(streams) if stream[3]]
+    cross_hops = (groups // 2, groups - 1 - groups // 2)
+    shares = n // groups
+
+    def carried(i, o, act):
+        if streams[i][3] and groups > 1:
+            pl.when(lax.rem(o, groups) == g)(act)
+        else:
+            act()
+
+    def cross_copy(i, o, way, k):
+        at, j = streams[i][1](o), split.index(i)
+        side = lax.rem(g + (1 if way == 0 else groups - 1), groups)
+        sems = (j, o // groups, way, k)
+        return rcopy(at, at, cross_send.at[sems], cross_recv.at[sems], {"grp": side})
+
+    def cross_class(way, k, incoming):
+        hop = k + incoming
+        return lax.rem(g + groups - hop, groups) if way == 0 else lax.rem(g + hop, groups)
+
+    def cross_each(i, k, incoming, act):
+        for way in (0, 1):
+            if k < cross_hops[way]:
+                for b in range(shares):
+                    o = b * groups + cross_class(way, k, incoming)
+                    pl.when(o != s)(functools.partial(act, i, o, way, k))
+
+    def cross_step(k):
+        def take(i, o, way, k):
+            cross_copy(i, o, way, k).wait_recv()
+            if k + 1 < cross_hops[way]:
+                cross_copy(i, o, way, k + 1).start()
+
+        for i in split:
+            cross_each(i, k, 1, take)
+
+    def cross_drain():
+        for i in split:
+            for k in range(cross_hops[0]):
+                cross_each(i, k, 0, lambda i, o, way, k: cross_copy(i, o, way, k).wait_send())
 
     def origin_out(way, k):
         return lax.rem(s + n - k, n) if way == 0 else lax.rem(s + k, n)
@@ -66,7 +117,7 @@
         return lax.rem(s + n - 1 - k, n) if way == 0 else lax.rem(s + 1 + k, n)
 
     def out_copy(i, way, k):
-        own, place, _ = streams[i]
+        own, place = streams[i][:2]
         at = place(origin_out(way, k))
         src = own if isinstance(k, int) and k == 0 else at
         return rcopy(src, at, ring_send.at[i, way, k], ring_recv.at[i, way, k], {"sp": nxt if way == 0 else prv})
@@ -79,24 +130,33 @@
         for i in group:
             for way in (0, 1):
                 if streams[i][2][way]:
-                    out_copy(i, way, 0).start()
+                    carried(i, s, out_copy(i, way, 0).start)
 
     def service(group, k):
         for i in group:
             for way in (0, 1):
                 hops = streams[i][2][way]
                 if k < hops:
-                    in_copy(i, way, k).wait_recv()
-                    if k + 1 < hops:
-                        out_copy(i, way, k + 1).start()
+                    o = origin_in(way, k)
+
+                    def pass_on(i=i, way=way, hops=hops, o=o):
+                        in_copy(i, way, k).wait_recv()
+                        if k + 1 < hops:
+                            out_copy(i, way, k + 1).start()
+                        if streams[i][3]:
+                            for across in (0, 1):
+                                if cross_hops[across]:
+                                    cross_copy(i, o, across, 0).start()
+
+                    carried(i, o, pass_on)
 
     def drain(group):
         for i in group:
             for way in (0, 1):
                 for k in range(streams[i][2][way]):
-                    out_copy(i, way, k).wait_send()
-
-    KV, GU, DN = (0, 1), (2, 3), (4, 5)
+                    carried(i, origin_out(way, k), out_copy(i, way, k).wait_send)
+
+    KV, GU, DN = (0, 1), (2, 3, 4), (5, 6)
 
     @pl.when(s < n - 1)
     def _():
@@ -133,7 +193,7 @@
                     z = lax.dot_general(
                         qtile, keys[pl.ds(c * kc, kc), :], (((1,), (1,)), ((), ())), preferred_element_type=F32
                     )
-                    soft = jnp.maximum(z, 0.0) + jnp.log(1.0 + jnp.exp(-jnp.abs(z)))
+                    soft = jnp.maximum(z, 0.0) + jnp.log(1.0 + jnp.exp2(jnp.abs(z) * -LOG2_E))
                     take = z - soft
                     if mode == "own":
                         key_pos = c * kc + lax.broadcasted_iota(jnp.int32, (qt, kc), 1)
@@ -190,6 +250,10 @@
         def _():
             start_group(GU)
 
+        @pl.when(k == far - 1)
+        def _():
+            service(GU, 0)
+
         @pl.when(up_need)
         def _():
             o = origin_in(0, k)
@@ -214,48 +278,112 @@
             att[...], wo_ref[:, pl.ds(c * nc, nc)], preferred_element_type=F32
         ).astype(BF16)
 
-    def rs_copy(d):
-        p = lax.rem(me + d, m)
-        return rcopy(
-            sbuf.at[pl.ds(pl.multiple_of(p * part, part), part), :], rbuf.at[d - 1],
-            rs_send.at[d - 1], rs_recv.at[d - 1], {"tp": p},
-        )
-
-    def ag_copy(d):
-        mine = x_all.at[pl.ds(pl.multiple_of(me * part, part), part), :]
-        return rcopy(mine, mine, ag_send.at[d - 1], ag_recv.at[d - 1], {"tp": lax.rem(me + d, m)})
-
-    def ag_in(d):
-        p = lax.rem(me + m - d, m)
-        at = x_all.at[pl.ds(pl.multiple_of(p * part, part), part), :]
-        return rcopy(at, at, ag_send.at[d - 1], ag_recv.at[d - 1], {"tp": p})
-
-    for d in range(1, m):
-        rs_copy(d).start()
+    n_x = m // 2
+    assert n_x == 4
+    x, core = me // 2, lax.rem(me, 2)
+    x_up, x_far, x_dn = lax.rem(x + 1, n_x), lax.rem(x + 2, n_x), lax.rem(x + 3, n_x)
+    mate = {"tp": 2 * x + 1 - core}
+    up_dev, dn_dev = {"tp": 2 * x_up + core}, {"tp": 2 * x_dn + core}
+    hp = part // 2
+    top, bottom = pl.ds(0, hp), pl.ds(hp, hp)
+
+    def rows_of(at_x, at_core, begin=0, size=part):
+        return pl.ds(pl.multiple_of((2 * at_x + at_core) * part + begin, size), size)
+
+    order = (x_far, x_up, x_dn, x)
+
+    def pair_copy(j):
+        return rcopy(sbuf.at[rows_of(order[j], 1 - core), :], pbuf.at[j], rs_send.at[j], rs_recv.at[j], mate)
+
+    far_up = rcopy(tbuf.at[0, top, :], hbuf.at[0], rs_send.at[4], rs_recv.at[4], up_dev)
+    far_dn = rcopy(tbuf.at[0, bottom, :], hbuf.at[1], rs_send.at[5], rs_recv.at[5], dn_dev)
+    raw_up = rcopy(tbuf.at[1, bottom, :], hbuf.at[2], rs_send.at[6], rs_recv.at[6], up_dev)
+    raw_dn = rcopy(tbuf.at[2, top, :], hbuf.at[3], rs_send.at[7], rs_recv.at[7], dn_dev)
+    sum_up = rcopy(cbuf.at[0], hbuf.at[4], rs_send.at[8], rs_recv.at[8], up_dev)
+    sum_dn = rcopy(cbuf.at[1], hbuf.at[5], rs_send.at[9], rs_recv.at[9], dn_dev)
+    rs_along = (far_up, far_dn, raw_up, raw_dn, sum_up, sum_dn)
+
+    def ag_to(i, at_x, device, begin=0, size=part):
+        at = x_all.at[rows_of(at_x, core, begin, size), :]
+        return rcopy(at, at, ag_send.at[i], ag_recv.at[i], device)
+
+    def ag_from(i, at_x, at_core, begin=0, size=part):
+        at = x_all.at[rows_of(at_x, at_core, begin, size), :]
+        return rcopy(at, at, ag_send.at[i], ag_recv.at[i], mate)
+
+    ag_out = [
+        ag_to(0, x, up_dev), ag_to(1, x, dn_dev), ag_to(2, x, mate),
+        ag_to(3, x_dn, up_dev, 0, hp), ag_to(4, x_dn, mate),
+        ag_to(5, x_up, dn_dev, hp, hp), ag_to(6, x_up, mate),
+        ag_to(7, x_far, mate, 0, hp), ag_to(8, x_far, mate, hp, hp),
+    ]
+    ag_in = [
+        ag_from(0, x_dn, core), ag_from(1, x_up, core), ag_from(2, x, 1 - core),
+        ag_from(3, x_far, core, 0, hp), ag_from(4, x_dn, 1 - core),
+        ag_from(5, x_far, core, hp, hp), ag_from(6, x_up, 1 - core),
+        ag_from(7, x_far, 1 - core, 0, hp), ag_from(8, x_far, 1 - core, hp, hp),
+    ]
 
     def norm(v, gain):
         mean_square = jnp.mean(v * v, axis=-1, keepdims=True)
         return v * lax.rsqrt(mean_square + norm_eps) * gain
 
-    third = (far + 1) // 3
-    for k in range(third):
-        service(GU, k)
-    for d in range(1, m):
-        rs_copy(d).wait()
-    mixed = sbuf[pl.ds(pl.multiple_of(me * part, part), part), :].astype(F32)
-    for d in range(1, m):
-        mixed = mixed + rbuf[d - 1].astype(F32)
+    def ring_step(j):
+        if j < far:
+            service(GU, j)
+
+    for j in range(4):
+        pair_copy(j).start()
+    ring_step(1)
+    for j in range(4):
+        pair_copy(j).wait_recv()
+        pair = sbuf[rows_of(order[j], core), :].astype(F32) + pbuf[j].astype(F32)
+        if j == 3:
+            first[...] = pair
+        else:
+            tbuf[j] = pair.astype(BF16)
+            for copy in ((far_up, far_dn), (raw_up,), (raw_dn,))[j]:
+                copy.start()
+    ring_step(2)
+    far_up.wait_recv()
+    cbuf[0] = (tbuf[1, top, :].astype(F32) + hbuf[0].astype(F32)).astype(BF16)
+    sum_up.start()
+    far_dn.wait_recv()
+    cbuf[1] = (tbuf[2, bottom, :].astype(F32) + hbuf[1].astype(F32)).astype(BF16)
+    sum_dn.start()
+    ring_step(3)
     res_copy.wait()
-    first[...] = res_v[...].astype(F32) + norm(mixed, pg_ref[...])
-    x_all[pl.ds(pl.multiple_of(me * part, part), part), :] = norm(first[...], prg_ref[...]).astype(BF16)
-    for d in range(1, m):
-        ag_copy(d).start()
-    for k in range(third, far):
-        if k == far - 1:
-            start_group(DN)
-        service(GU, k)
-    for d in range(1, m):
-        ag_in(d).wait_recv()
+    for copy in (raw_up, raw_dn, sum_up, sum_dn):
+        copy.wait_recv()
+    for half, (raw, summed) in ((top, (3, 4)), (bottom, (2, 5))):
+        mixed = first[half, :] + hbuf[raw].astype(F32) + hbuf[summed].astype(F32)
+        first[half, :] = res_v[half, :].astype(F32) + norm(mixed, pg_ref[...])
+    x_all[rows_of(x, core), :] = norm(first[...], prg_ref[...]).astype(BF16)
+    for i in (0, 1, 2):
+        ag_out[i].start()
+    ring_step(4)
+    ag_in[0].wait_recv()
+    for i in (3, 4):
+        ag_out[i].start()
+    ag_in[1].wait_recv()
+    for i in (5, 6):
+        ag_out[i].start()
+    ring_step(5)
+    ag_in[3].wait_recv()
+    ag_out[7].start()
+    ag_in[5].wait_recv()
+    ag_out[8].start()
+    start_group(DN)
+    for k in range(6, far):
+        ring_step(k)
+    early = min(far, max(1, cross_hops[0] - 1))
+    for k in range(max(early, cross_hops[0])):
+        if k < early:
+            service(DN, k)
+        if k < cross_hops[0]:
+            cross_step(k)
+    for i in (2, 4, 6, 7, 8):
+        ag_in[i].wait_recv()
 
     mt = min(256, toks)
 
@@ -280,8 +408,22 @@
             return [s]
         return [origin_in(way, c - 1) for way in (0, 1) if c - 1 < streams[DN[0]][2][way]]
 
+    def finish(c, square):
+        origins = chunk_origins(c)
+        wide = cols * len(origins)
+        for d in range(1, m):
+            fs_copy(c, wide, d).wait()
+        total = fbuf[c, pl.ds(pl.multiple_of(me * part, part), part), pl.ds(0, wide)].astype(F32)
+        for d in range(1, m):
+            total = total + rb[c, d - 1, :, pl.ds(0, wide)].astype(F32)
+        for j, o in enumerate(origins):
+            ff[o] = total[:, j * cols : (j + 1) * cols]
+        return square + jnp.sum(total * total, axis=-1, keepdims=True)
+
+    square = jnp.zeros((part, 1), F32)
+    behind = 3
     for c in range(far + 1):
-        if c:
+        if c > early:
             service(DN, c - 1)
         origins = chunk_origins(c)
         tiles = [down_ref[...] if c == 0 else dall[o] for o in origins]
@@ -290,26 +432,21 @@
         fbuf[c, :, pl.ds(0, wide)] = jnp.dot(hidden[...], both, preferred_element_type=F32).astype(BF16)
         for d in range(1, m):
             fs_copy(c, wide, d).start()
-
-    square = jnp.zeros((part, 1), F32)
-    for c in range(far + 1):
-        origins = chunk_origins(c)
-        wide = cols * len(origins)
-        for d in range(1, m):
-            fs_copy(c, wide, d).wait()
-        total = fbuf[c, pl.ds(pl.multiple_of(me * part, part), part), pl.ds(0, wide)].astype(F32)
-        for d in range(1, m):
-            total = total + rb[c, d - 1, :, pl.ds(0, wide)].astype(F32)
-        square = square + jnp.sum(total * total, axis=-1, keepdims=True)
-        for j, o in enumerate(origins):
-            ff[o] = total[:, j * cols : (j + 1) * cols]
+        if c >= behind:
+            square = finish(c - behind, square)
+    for c in range(max(0, far + 1 - behind), far + 1):
+        square = finish(c, square)
     scale = lax.rsqrt(square / d_model + norm_eps)
     for o in range(n):
         at = pl.ds(o * cols, cols)
         out_ref[:, at] = (first[:, at] + 0.5 * (ff[o] * scale * fg_ref[:, at])).astype(out_ref.dtype)
 
-    for d in range(1, m):
-        ag_copy(d).wait_send()
+    for j in range(4):
+        pair_copy(j).wait_send()
+    for copy in rs_along:
+        copy.wait_send()
+    for copy in ag_out:
+        copy.wait_send()
 
     def kv_drain(k, carry_in):
         for i in KV:
@@ -325,11 +462,12 @@
 
     lax.fori_loop(0, far, kv_drain, 0)
     drain(GU)
+    cross_drain()
     drain(DN)
 
 
 def solution(mesh):
-    n, m = mesh.shape["sp"], mesh.shape["tp"]
+    groups, n, m = mesh.shape["grp"], mesh.shape["sp"], mesh.shape["tp"]
 
     def per_device(q, k, v, residual, wo, pg, gate, up, down, prg, fg):
         toks, width = q.shape
@@ -347,7 +485,7 @@
         specs[3] = pl.BlockSpec(memory_space=pl.ANY)
         flops = 2 * toks * (n * toks * width * 4 + width * d_model + 3 * d_model * f_loc)
         return pl.pallas_call(
-            functools.partial(layer_kernel, n, m),
+            functools.partial(layer_kernel, groups, n, m),
             out_shape=jax.ShapeDtypeStruct((part, d_model), BF16),
             in_specs=specs,
             out_specs=in_vmem,
@@ -364,7 +502,10 @@
                 vm((heads, toks, 1), F32),
                 vm((toks, width), BF16),
                 vm((toks, d_model), BF16),
-                vm((m - 1, part, d_model), BF16),
+                vm((4, part, d_model), BF16),
+                vm((3, part, d_model), BF16),
+                vm((6, part // 2, d_model), BF16),
+                vm((2, part // 2, d_model), BF16),
                 vm((part, d_model), BF16),
                 vm((part, d_model), F32),
                 vm((toks, d_model), BF16),
@@ -372,12 +513,14 @@
                 vm((chunks, toks, 2 * cols), BF16),
                 vm((chunks, m - 1, part, 2 * cols), BF16),
                 vm((n, part, cols), F32),
-                dma((6, 2, far)),
-                dma((6, 2, far)),
-                dma((m - 1,)),
-                dma((m - 1,)),
-                dma((m - 1,)),
-                dma((m - 1,)),
+                dma((7, 2, far)),
+                dma((7, 2, far)),
+                dma((2, n // groups, 2, max(1, groups // 2))),
+                dma((2, n // groups, 2, max(1, groups // 2))),
+                dma((10,)),
+                dma((10,)),
+                dma((9,)),
+                dma((9,)),
                 dma((chunks, m - 1)),
                 dma((chunks, m - 1)),
                 dma,

time: 190 us -> 170 us (0.89)
  Pallas kernels: 188 us -> 168 us
    pallas_call x1, Pallas kernels: 188 us -> 168 us  [per_device(): pl.pallas_call(functools.partial(layer_kernel, groups, n, m), out_shape=j...]
where the time goes in v2:
time: 170 us
  Pallas kernels  168 us (99%)
    pallas_call x1, Pallas kernels, per_device(): pl.pallas_call(functools.partial(layer_kernel, groups, n, m), out_shape=j...  168 us

profile of v2, /device:TPU:33, one launch (start us, length us, event | category | flops | bytes accessed | tf_op | source)
XLA Modules:
  0.0 170.1 jit_solution(16338180906970015345)
XLA Ops:
  0.0 168.4 %shard_map.109 = bf16[64,2048]{1,0:T(8,128)(2,1)} custom-call(bf16[512,128]{1,0:T(8,128)(2,1)} %q_ref.1, bf16[512,128]{1,0:T(8,128)(2,1)} %k_ref.1, bf16[512,128]{1,0:T(8,128)(2,1)} %v_ref.1, bf16[512,2048]{1,0:T(8,128)(2,1)} %res_ref.1, bf16[128,2048]{1,0:T(8,128)(2,1)} %wo_ref.1, f32[1,2048]{1,0:T(1,128)} %bitcast.3, bf16[128,640]{1,0:T(8,128)(2,1)} %gate_ref.1, ...), custom_call_target="tpu_custom_call" | custom-call | flops 8589934592 | bytes 4194304 | tf_op jit(solution)/shard_map/pallas_call | solution.py:487
  168.4 1.7 copy.13

commit v3 on v2

--- a/solution.py
+++ b/solution.py
@@ -9,6 +9,7 @@
 
 HEAD_DIM = 64
 norm_eps = 1e-06
+N_COL_GROUPS = 3
 LOG2_E = 1.4426950408889634
 MESH = pl.DeviceIdType.MESH
 F32 = jnp.float32
@@ -27,7 +28,7 @@
     q_ref, k_ref, v_ref, res_ref, wo_ref, pg_ref, gate_ref, up_ref, down_ref, prg_ref, fg_ref,
     out_ref,
     kall, vall, gall, uall, dall, qm, tri, acc, acc_low, lost, att, sbuf, pbuf, tbuf, hbuf, cbuf, res_v, first, x_all, hidden,
-    fbuf, rb, ff,
+    fbuf, pb, tb, hb, cb, kept, ff,
     ring_send, ring_recv, cross_send, cross_recv, rs_send, rs_recv, ag_send, ag_recv, fs_send, fs_recv, res_sem,
 ):
     g = lax.axis_index("grp")
@@ -42,7 +43,7 @@
     d_model = wo_ref.shape[1]
     part = toks // m
     kc = min(256, toks)
-    qt = min(256, toks)
+    qt = min(512, toks)
     near, far = n // 2 - 1, n // 2
 
     barrier = pltpu.get_barrier_semaphore()
@@ -292,16 +293,55 @@
 
     order = (x_far, x_up, x_dn, x)
 
-    def pair_copy(j):
-        return rcopy(sbuf.at[rows_of(order[j], 1 - core), :], pbuf.at[j], rs_send.at[j], rs_recv.at[j], mate)
-
-    far_up = rcopy(tbuf.at[0, top, :], hbuf.at[0], rs_send.at[4], rs_recv.at[4], up_dev)
-    far_dn = rcopy(tbuf.at[0, bottom, :], hbuf.at[1], rs_send.at[5], rs_recv.at[5], dn_dev)
-    raw_up = rcopy(tbuf.at[1, bottom, :], hbuf.at[2], rs_send.at[6], rs_recv.at[6], up_dev)
-    raw_dn = rcopy(tbuf.at[2, top, :], hbuf.at[3], rs_send.at[7], rs_recv.at[7], dn_dev)
-    sum_up = rcopy(cbuf.at[0], hbuf.at[4], rs_send.at[8], rs_recv.at[8], up_dev)
-    sum_dn = rcopy(cbuf.at[1], hbuf.at[5], rs_send.at[9], rs_recv.at[9], dn_dev)
-    rs_along = (far_up, far_dn, raw_up, raw_dn, sum_up, sum_dn)
+    class Sum:
+        def __init__(self, src, pairs, sums, halves, joint, kept, send, recv):
+            self.src, self.pairs, self.sums, self.halves, self.joint, self.kept = src, pairs, sums, halves, joint, kept
+            self.pair = [rcopy(src(rows_of(order[j], 1 - core)), pairs(j), send(j), recv(j), mate) for j in range(4)]
+            self.along = [
+                rcopy(sums(0, top), halves(0), send(4), recv(4), up_dev),
+                rcopy(sums(0, bottom), halves(1), send(5), recv(5), dn_dev),
+                rcopy(sums(1, bottom), halves(2), send(6), recv(6), up_dev),
+                rcopy(sums(2, top), halves(3), send(7), recv(7), dn_dev),
+                rcopy(joint(0), halves(4), send(8), recv(8), up_dev),
+                rcopy(joint(1), halves(5), send(9), recv(9), dn_dev),
+            ]
+
+        def to_mate(self):
+            for copy in self.pair:
+                copy.start()
+
+        def join_pair(self):
+            for j in range(4):
+                self.pair[j].wait_recv()
+                pair = self.src(rows_of(order[j], core))[...].astype(F32) + self.pairs(j)[...].astype(F32)
+                if j == 3:
+                    self.kept[...] = pair
+                else:
+                    self.sums(j, pl.ds(0, part))[...] = pair.astype(BF16)
+                    for i in ((0, 1), (2,), (3,))[j]:
+                        self.along[i].start()
+
+        def pass_far(self):
+            for i, j, half in ((0, 1, top), (1, 2, bottom)):
+                self.along[i].wait_recv()
+                both = self.sums(j, half)[...].astype(F32) + self.halves(i)[...].astype(F32)
+                self.joint(i)[...] = both.astype(BF16)
+                self.along[4 + i].start()
+
+        def result(self):
+            for i in (2, 3, 4, 5):
+                self.along[i].wait_recv()
+            for half, raw, summed in ((top, 3, 4), (bottom, 2, 5)):
+                yield half, self.kept[half, :] + self.halves(raw)[...].astype(F32) + self.halves(summed)[...].astype(F32)
+
+        def sent(self):
+            for copy in self.pair + self.along:
+                copy.wait_send()
+
+    mix = Sum(
+        lambda r: sbuf.at[r, :], lambda j: pbuf.at[j], lambda j, r: tbuf.at[j, r, :], lambda i: hbuf.at[i],
+        lambda i: cbuf.at[i], first, lambda i: rs_send.at[i], lambda i: rs_recv.at[i],
+    )
 
     def ag_to(i, at_x, device, begin=0, size=part):
         at = x_all.at[rows_of(at_x, core, begin, size), :]
@@ -328,35 +368,24 @@
         mean_square = jnp.mean(v * v, axis=-1, keepdims=True)
         return v * lax.rsqrt(mean_square + norm_eps) * gain
 
+    lag = 2
+
     def ring_step(j):
         if j < far:
             service(GU, j)
-
-    for j in range(4):
-        pair_copy(j).start()
+        if j == lag - 1:
+            start_group(DN)
+        if j >= lag:
+            service(DN, j - lag)
+
+    mix.to_mate()
     ring_step(1)
-    for j in range(4):
-        pair_copy(j).wait_recv()
-        pair = sbuf[rows_of(order[j], core), :].astype(F32) + pbuf[j].astype(F32)
-        if j == 3:
-            first[...] = pair
-        else:
-            tbuf[j] = pair.astype(BF16)
-            for copy in ((far_up, far_dn), (raw_up,), (raw_dn,))[j]:
-                copy.start()
+    mix.join_pair()
     ring_step(2)
-    far_up.wait_recv()
-    cbuf[0] = (tbuf[1, top, :].astype(F32) + hbuf[0].astype(F32)).astype(BF16)
-    sum_up.start()
-    far_dn.wait_recv()
-    cbuf[1] = (tbuf[2, bottom, :].astype(F32) + hbuf[1].astype(F32)).astype(BF16)
-    sum_dn.start()
+    mix.pass_far()
     ring_step(3)
     res_copy.wait()
-    for copy in (raw_up, raw_dn, sum_up, sum_dn):
-        copy.wait_recv()
-    for half, (raw, summed) in ((top, (3, 4)), (bottom, (2, 5))):
-        mixed = first[half, :] + hbuf[raw].astype(F32) + hbuf[summed].astype(F32)
+    for half, mixed in mix.result():
         first[half, :] = res_v[half, :].astype(F32) + norm(mixed, pg_ref[...])
     x_all[rows_of(x, core), :] = norm(first[...], prg_ref[...]).astype(BF16)
     for i in (0, 1, 2):
@@ -373,13 +402,13 @@
     ag_out[7].start()
     ag_in[5].wait_recv()
     ag_out[8].start()
-    start_group(DN)
     for k in range(6, far):
         ring_step(k)
-    early = min(far, max(1, cross_hops[0] - 1))
-    for k in range(max(early, cross_hops[0])):
-        if k < early:
-            service(DN, k)
+    done = far - lag
+    early = min(far, max(done + 1, cross_hops[0] - 1))
+    for k in range(max(early - done, cross_hops[0])):
+        if done + k < early:
+            service(DN, done + k)
         if k < cross_hops[0]:
             cross_step(k)
     for i in (2, 4, 6, 7, 8):
@@ -396,55 +425,54 @@
 
     lax.fori_loop(0, toks // mt, ffn_tile, 0)
 
-    def fs_copy(c, wide, d):
-        p = lax.rem(me + d, m)
-        return rcopy(
-            fbuf.at[c, pl.ds(pl.multiple_of(p * part, part), part), pl.ds(0, wide)], rb.at[c, d - 1, :, pl.ds(0, wide)],
-            fs_send.at[c, d - 1], fs_recv.at[c, d - 1], {"tp": p},
-        )
-
-    def chunk_origins(c):
+    def origins_of(c):
         if c == 0:
             return [s]
         return [origin_in(way, c - 1) for way in (0, 1) if c - 1 < streams[DN[0]][2][way]]
 
-    def finish(c, square):
-        origins = chunk_origins(c)
-        wide = cols * len(origins)
-        for d in range(1, m):
-            fs_copy(c, wide, d).wait()
-        total = fbuf[c, pl.ds(pl.multiple_of(me * part, part), part), pl.ds(0, wide)].astype(F32)
-        for d in range(1, m):
-            total = total + rb[c, d - 1, :, pl.ds(0, wide)].astype(F32)
-        for j, o in enumerate(origins):
-            ff[o] = total[:, j * cols : (j + 1) * cols]
-        return square + jnp.sum(total * total, axis=-1, keepdims=True)
-
-    square = jnp.zeros((part, 1), F32)
-    behind = 3
-    for c in range(far + 1):
-        if c > early:
-            service(DN, c - 1)
-        origins = chunk_origins(c)
-        tiles = [down_ref[...] if c == 0 else dall[o] for o in origins]
-        wide = cols * len(tiles)
-        both = tiles[0] if len(tiles) == 1 else jnp.concatenate(tiles, axis=1)
-        fbuf[c, :, pl.ds(0, wide)] = jnp.dot(hidden[...], both, preferred_element_type=F32).astype(BF16)
-        for d in range(1, m):
-            fs_copy(c, wide, d).start()
-        if c >= behind:
-            square = finish(c - behind, square)
-    for c in range(max(0, far + 1 - behind), far + 1):
-        square = finish(c, square)
+    size = -(-(far + 1) // N_COL_GROUPS)
+    members = [list(range(i, min(i + size, far + 1))) for i in range(0, far + 1, size)]
+    origins = [[o for c in chunk for o in origins_of(c)] for chunk in members]
+
+    def column_sum(q):
+        wide = pl.ds(0, cols * len(origins[q]))
+        return Sum(
+            lambda r: fbuf.at[q, r, wide], lambda j: pb.at[q, j, :, wide], lambda j, r: tb.at[q, j, r, wide],
+            lambda i: hb.at[q, i, :, wide], lambda i: cb.at[q, i, :, wide], kept.at[q, :, wide],
+            lambda i: fs_send.at[q, i], lambda i: fs_recv.at[q, i],
+        )
+
+    col_sums = [column_sum(q) for q in range(len(members))]
+    square = [jnp.zeros((hp, 1), F32), jnp.zeros((hp, 1), F32)]
+    for step in range(len(members) + 3):
+        if step < len(members):
+            at = 0
+            for c in members[step]:
+                if c > early:
+                    service(DN, c - 1)
+                tiles = [down_ref[...] if c == 0 else dall[o] for o in origins_of(c)]
+                both = tiles[0] if len(tiles) == 1 else jnp.concatenate(tiles, axis=1)
+                wide = cols * len(tiles)
+                fbuf[step, :, pl.ds(at, wide)] = jnp.dot(hidden[...], both, preferred_element_type=F32).astype(BF16)
+                at += wide
+            col_sums[step].to_mate()
+        if 0 <= step - 1 < len(members):
+            col_sums[step - 1].join_pair()
+        if 0 <= step - 2 < len(members):
+            col_sums[step - 2].pass_far()
+        if 0 <= step - 3 < len(members):
+            for i, (half, total) in enumerate(col_sums[step - 3].result()):
+                square[i] = square[i] + jnp.sum(total * total, axis=-1, keepdims=True)
+                for j, o in enumerate(origins[step - 3]):
+                    ff[o, half, :] = total[:, j * cols : (j + 1) * cols]
+    square = jnp.concatenate(square, axis=0)
     scale = lax.rsqrt(square / d_model + norm_eps)
     for o in range(n):
         at = pl.ds(o * cols, cols)
         out_ref[:, at] = (first[:, at] + 0.5 * (ff[o] * scale * fg_ref[:, at])).astype(out_ref.dtype)
 
-    for j in range(4):
-        pair_copy(j).wait_send()
-    for copy in rs_along:
-        copy.wait_send()
+    for total in (mix, *col_sums):
+        total.sent()
     for copy in ag_out:
         copy.wait_send()
 
@@ -477,7 +505,8 @@
         part = toks // m
         cols = down.shape[1]
         far = n // 2
-        chunks = far + 1
+        size = -(-(far + 1) // N_COL_GROUPS)
+        col_groups, wide = -(-(far + 1) // size), 2 * size * cols
         kc = min(256, toks)
         vm, dma = pltpu.VMEM, pltpu.SemaphoreType.DMA
         in_vmem = pl.BlockSpec(memory_space=vm)
@@ -510,8 +539,12 @@
                 vm((part, d_model), F32),
                 vm((toks, d_model), BF16),
                 vm((toks, f_loc), BF16),
-                vm((chunks, toks, 2 * cols), BF16),
-                vm((chunks, m - 1, part, 2 * cols), BF16),
+                vm((col_groups, toks, wide), BF16),
+                vm((col_groups, 4, part, wide), BF16),
+                vm((col_groups, 3, part, wide), BF16),
+                vm((col_groups, 6, part // 2, wide), BF16),
+                vm((col_groups, 2, part // 2, wide), BF16),
+                vm((col_groups, part, wide), F32),
                 vm((n, part, cols), F32),
                 dma((7, 2, far)),
                 dma((7, 2, far)),
@@ -521,8 +554,8 @@
                 dma((10,)),
                 dma((9,)),
                 dma((9,)),
-                dma((chunks, m - 1)),
-                dma((chunks, m - 1)),
+                dma((col_groups, 10)),
+                dma((col_groups, 10)),
                 dma,
             ],
             compiler_params=pltpu.CompilerParams(

time: 170 us -> 157 us (0.924)
  Pallas kernels: 168 us -> 156 us
    pallas_call x1, Pallas kernels: 168 us -> 156 us  [per_device(): pl.pallas_call(functools.partial(layer_kernel, groups, n, m), out_shape=j...]
where the time goes in v3:
time: 157 us
  Pallas kernels  156 us (99%)
  local copies, waits for them, and re-layouts  1.67 us (1%)
    pallas_call x1, Pallas kernels, per_device(): pl.pallas_call(functools.partial(layer_kernel, groups, n, m), out_shape=j...  156 us

profile of v3, /device:TPU:33, one launch (start us, length us, event | category | flops | bytes accessed | tf_op | source)
XLA Modules:
  0.0 157.3 jit_solution(12183932719450428136)
XLA Ops:
  0.0 155.6 %shard_map.109 = bf16[64,2048]{1,0:T(8,128)(2,1)} custom-call(bf16[512,128]{1,0:T(8,128)(2,1)} %q_ref.1, bf16[512,128]{1,0:T(8,128)(2,1)} %k_ref.1, bf16[512,128]{1,0:T(8,128)(2,1)} %v_ref.1, bf16[512,2048]{1,0:T(8,128)(2,1)} %res_ref.1, bf16[128,2048]{1,0:T(8,128)(2,1)} %wo_ref.1, f32[1,2048]{1,0:T(1,128)} %bitcast.3, bf16[128,640]{1,0:T(8,128)(2,1)} %gate_ref.1, ...), custom_call_target="tpu_custom_call" | custom-call | flops 8589934592 | bytes 4194304 | tf_op jit(solution)/shard_map/pallas_call | solution.py:516
  155.6 1.7 %copy.13 = bf16[64,2048]{1,0:T(8,128)(2,1)} copy(bf16[64,2048]{1,0:T(8,128)(2,1)} %shard_map.109) | data formatting | bytes 524288

commit v4 on v3

--- a/solution.py
+++ b/solution.py
@@ -9,7 +9,7 @@
 
 HEAD_DIM = 64
 norm_eps = 1e-06
-N_COL_GROUPS = 3
+N_COL_GROUPS = 5
 LOG2_E = 1.4426950408889634
 MESH = pl.DeviceIdType.MESH
 F32 = jnp.float32
@@ -368,7 +368,7 @@
         mean_square = jnp.mean(v * v, axis=-1, keepdims=True)
         return v * lax.rsqrt(mean_square + norm_eps) * gain
 
-    lag = 2
+    lag = 3
 
     def ring_step(j):
         if j < far:

time: 157 us -> 163 us (1.038)
  Pallas kernels: 156 us -> 160 us
    pallas_call x1, Pallas kernels: 156 us -> 160 us  [per_device(): pl.pallas_call(functools.partial(layer_kernel, groups, n, m), out_shape=j...]
where the time goes in v4:
time: 163 us; the launch traced here: 162 us
  Pallas kernels  160 us (98%)
  local copies, waits for them, and re-layouts  1.67 us (1%)
    pallas_call x1, Pallas kernels, per_device(): pl.pallas_call(functools.partial(layer_kernel, groups, n, m), out_shape=j...  160 us

profile of v4, /device:TPU:33, one launch (start us, length us, event | category | flops | bytes accessed | tf_op | source)
XLA Modules:
  0.0 162.1 jit_solution(7302559124741611689)
XLA Ops:
  0.0 160.5 %shard_map.109 = bf16[64,2048]{1,0:T(8,128)(2,1)} custom-call(bf16[512,128]{1,0:T(8,128)(2,1)} %q_ref.1, bf16[512,128]{1,0:T(8,128)(2,1)} %k_ref.1, bf16[512,128]{1,0:T(8,128)(2,1)} %v_ref.1, bf16[512,2048]{1,0:T(8,128)(2,1)} %res_ref.1, bf16[128,2048]{1,0:T(8,128)(2,1)} %wo_ref.1, f32[1,2048]{1,0:T(1,128)} %bitcast.3, bf16[128,640]{1,0:T(8,128)(2,1)} %gate_ref.1, ...), custom_call_target="tpu_custom_call" | custom-call | flops 8589934592 | bytes 4194304 | tf_op jit(solution)/shard_map/pallas_call | solution.py:516
  160.5 1.7 %copy.13 = bf16[64,2048]{1,0:T(8,128)(2,1)} copy(bf16[64,2048]{1,0:T(8,128)(2,1)} %shard_map.109) | data formatting | bytes 524288
